TPU v7x, 32 devices: a whole 2x2x4 slice. The times are simulated.
32 devices in a mesh: fs: 8 (over z, y), tp: 4 (over x, core).
Axes of the slice: x: 2, y: 2, z: 4, core: 2. Of those that a mesh axis runs over, the one named last changes fastest.
Arguments:
- stream_in: bfloat16 [2048, 2112], P('fs'), may hold values from -6 to 6
- norm_gains: float32 [6, 2112], replicated, may hold values from 0.1 to 1.9
- gate_proj: bfloat16 [2112, 3072], P('fs', 'tp'), may hold values from -0.125 to 0.125
- up_proj: bfloat16 [2112, 3072], P('fs', 'tp'), may hold values from -0.125 to 0.125
- down_proj: bfloat16 [2112, 3072], P('fs', 'tp'), may hold values from -0.109375 to 0.109375
- outer_gate: bfloat16 [2112, 1056], P('fs', 'tp'), may hold values from -0.125 to 0.125
- inner_gate: bfloat16 [2112, 1056], P('fs', 'tp'), may hold values from -0.125 to 0.125
- value_proj: bfloat16 [2112, 1056], P('fs', 'tp'), may hold values from -0.125 to 0.125
- mixer_out: bfloat16 [2112, 1056], P('fs', 'tp'), may hold values from -0.1875 to 0.1875
- conv_taps: bfloat16 [3, 1056], replicated, may hold values from -3 to 3
Outputs:
- stream_out: bfloat16 [2048, 2112], P('fs')
All inputs are finite; a program needn't handle non-finite values.
Results may differ from a plain program's by a relative error of at most 0.02.
Values may be sent and summed in bfloat16 or wider, within the bound.
A program may use at most 64 MiB of HBM per device.

v0:
```python
import jax
import jax.numpy as jnp
from jax import lax
from jax.sharding import PartitionSpec as P

CONV_K = 3


EPSILON = 1e-06


def scaled(values, gain):
    return values * lax.rsqrt(jnp.mean(values * values, axis=-1, keepdims=True) + EPSILON) * gain


def narrow(inner, weight, stream, gain, factor):
    partial_value = lax.dot_general(
        inner, weight, (((1,), (1,)), ((), ())), preferred_element_type=jnp.float32
    )
    summed = lax.psum(partial_value.astype(jnp.bfloat16), "tp").astype(jnp.float32)
    return (stream.astype(jnp.float32) + factor * scaled(summed, gain)).astype(jnp.bfloat16)


def half_step(stream, weights, pre_gain, post_gain):
    gate_full, up_full, down_full = weights
    normed = scaled(stream.astype(jnp.float32), pre_gain).astype(jnp.bfloat16)
    gate = jnp.dot(normed, gate_full, preferred_element_type=jnp.float32)
    upward = jnp.dot(normed, up_full, preferred_element_type=jnp.float32)
    hidden = (jax.nn.silu(gate) * upward).astype(jnp.bfloat16)
    return narrow(hidden, down_full, stream, post_gain, 0.5)


def mixer_step(stream, weights, conv_taps, pre_gain, post_gain):
    outer_full, inner_full, value_full, out_full = weights
    channels = outer_full.shape[1]
    normed = scaled(stream.astype(jnp.float32), pre_gain).astype(jnp.bfloat16)
    outer = (
        jnp.dot(normed, outer_full, preferred_element_type=jnp.float32)
        .astype(jnp.bfloat16)
        .astype(jnp.float32)
    )
    inner = (
        jnp.dot(normed, inner_full, preferred_element_type=jnp.float32)
        .astype(jnp.bfloat16)
        .astype(jnp.float32)
    )
    value = (
        jnp.dot(normed, value_full, preferred_element_type=jnp.float32)
        .astype(jnp.bfloat16)
        .astype(jnp.float32)
    )
    gated = inner * value
    taps = lax.dynamic_slice_in_dim(conv_taps, lax.axis_index("tp") * channels, channels, 1).astype(
        jnp.float32
    )
    length = gated.shape[0]
    padded = jnp.concatenate([jnp.zeros((CONV_K - 1, channels), jnp.float32), gated], axis=0)
    conv = jnp.zeros_like(gated)
    for offset in range(CONV_K):
        conv = conv + taps[offset] * padded[offset : offset + length]
    mixed = (outer * conv).astype(jnp.bfloat16)
    return narrow(mixed, out_full, stream, post_gain, 1.0)


def local(
    stream_in,
    norm_gains,
    gate_proj,
    up_proj,
    down_proj,
    outer_gate,
    inner_gate,
    value_proj,
    mixer_out,
    conv_taps,
):
    mlp_full = (
        lax.all_gather(gate_proj, "fs", axis=0, tiled=True),
        lax.all_gather(up_proj, "fs", axis=0, tiled=True),
        lax.all_gather(down_proj, "fs", axis=0, tiled=True),
    )
    mixer_full = None
    stream = half_step(stream_in, mlp_full, norm_gains[0], norm_gains[1])
    mixer_full = (
        lax.all_gather(outer_gate, "fs", axis=0, tiled=True),
        lax.all_gather(inner_gate, "fs", axis=0, tiled=True),
        lax.all_gather(value_proj, "fs", axis=0, tiled=True),
        lax.all_gather(mixer_out, "fs", axis=0, tiled=True),
    )
    stream = mixer_step(stream, mixer_full, conv_taps, norm_gains[2], norm_gains[3])
    return half_step(stream, mlp_full, norm_gains[4], norm_gains[5])


def solution(mesh):
    return jax.shard_map(
        local,
        mesh=mesh,
        in_specs=(
            P("fs", None),
            P(),
            P("fs", "tp"),
            P("fs", "tp"),
            P("fs", "tp"),
            P("fs", "tp"),
            P("fs", "tp"),
            P("fs", "tp"),
            P("fs", "tp"),
            P(),
        ),
        out_specs=P("fs", None),
        check_vma=False,
    )
```

profile of v0, /device:TPU:0, one launch (start us, length us, event | category | flops | bytes accessed | tf_op | source)
XLA Modules:
  0.0 522.5 jit_solution(16457004554758750413)
XLA Ops:
  6.5 0.0 all-gather.8.cloned.1.call-start
  6.5 0.7 all-gather.8.cloned.1.call-update
  7.3 0.0 all-gather.10.cloned.1.call-start
  7.3 0.7 all-gather.10.cloned.1.call-update
  8.0 0.0 all-gather.12.cloned.1.call-start
  8.1 0.7 all-gather.12.cloned.1.call-update
  8.7 0.0 all-reduce.5.cloned.1.call-start
  8.8 1.4 slice_reduce_fusion
  10.2 1.6 fusion.8
  11.8 61.5 %all-gather.8.cloned.1.call-done = bf16[2112,768]{1,0:T(8,128)(2,1)} async-done(((bf16[264,768]{1,0:T(8,128)(2,1)}), bf16[2112,768]{1,0:T(8,128)(2,1)}) %all-gather.8.cloned.1.call-update) | async-done | bytes 3244048 | tf_op jit(solution)/shard_map/all_gather | solution.py:78
  73.3 0.0 copy-done
  73.3 3.2 fusion.36
  76.6 58.7 %all-gather.10.cloned.1.call-done = bf16[2112,768]{1,0:T(8,128)(2,1)} async-done(((bf16[264,768]{1,0:T(8,128)(2,1)}), bf16[2112,768]{1,0:T(8,128)(2,1)}) %all-gather.10.cloned.1.call-update) | async-done | bytes 3244048 | tf_op jit(solution)/shard_map/all_gather | solution.py:79
  135.3 62.0 %all-gather.12.cloned.1.call-done = bf16[2112,768]{1,0:T(8,128)(2,1)} async-done(((bf16[264,768]{1,0:T(8,128)(2,1)}), bf16[2112,768]{1,0:T(8,128)(2,1)}) %all-gather.12.cloned.1.call-update) | async-done | bytes 3244048 | tf_op jit(solution)/shard_map/all_gather | solution.py:80
  197.2 6.6 %convolution_convert_fusion.2 = bf16[256,2112]{0,1:T(8,128)(2,1)} fusion(bf16[2112,768]{1,0:T(8,128)(2,1)} %all-gather.12.cloned.1.call-done, bf16[2112,768]{1,0:T(8,128)(2,1)} %all-gather.10.cloned.1.call-done, f32[256,768]{1,0:T(8,128)S(1)} %fusion.36, bf16[256,2112]{0,1:T(8,128)(2,1)S(1)} %copy-done, f32[2112]{0:T(1024)S(1)} %get-tuple-element.9, ...), kind=kOutput, calls=%fused_computation.2 | convolution fusion | flops 1664827392 | bytes 9446656 | tf_op jit(solution)/shard_map/dot_general | solution.py:17
  203.9 0.0 all-reduce.5.cloned.1.call-update
  203.9 0.0 all-gather.16.cloned.1.call-start
  203.9 0.5 all-gather.16.cloned.1.call-update
  204.5 0.0 all-gather.18.cloned.1.call-start
  204.5 0.5 all-gather.18.cloned.1.call-update
  205.0 0.0 all-gather.14.cloned.1.call-start
  205.1 0.7 all-gather.14.cloned.1.call-update
  205.8 0.0 all-gather.20.cloned.1.call-start
  205.8 0.7 all-gather.20.cloned.1.call-update
  206.5 0.0 all-reduce.7.cloned.1.call-start
  206.6 0.8 dynamic-slice_convert_fusion
  207.4 32.0 %all-reduce.5.cloned.1.call-done = bf16[256,2112]{0,1:T(8,128)(2,1)} async-done(((bf16[256,2112]{0,1:T(8,128)(2,1)}), bf16[256,2112]{0,1:T(8,128)(2,1)}) %all-reduce.5.cloned.1.call-update) | async-done | bytes 1081360 | tf_op jit(solution)/shard_map/psum | solution.py:20
  239.4 1.5 fusion
  241.0 1.9 fusion.12
  242.9 43.7 %all-gather.16.cloned.1.call-done = bf16[2112,264]{1,0:T(8,128)(2,1)} async-done(((bf16[264,264]{1,0:T(8,128)(2,1)}), bf16[2112,264]{1,0:T(8,128)(2,1)}) %all-gather.16.cloned.1.call-update) | async-done | bytes 1115152 | tf_op jit(solution)/shard_map/all_gather | solution.py:86
  286.6 2.5 fusion.24
  289.0 42.7 %all-gather.18.cloned.1.call-done = bf16[2112,264]{1,0:T(8,128)(2,1)} async-done(((bf16[264,264]{1,0:T(8,128)(2,1)}), bf16[2112,264]{1,0:T(8,128)(2,1)}) %all-gather.18.cloned.1.call-update) | async-done | bytes 1115152 | tf_op jit(solution)/shard_map/all_gather | solution.py:87
  331.7 2.5 fusion.23
  334.2 42.9 %all-gather.14.cloned.1.call-done = bf16[2112,264]{1,0:T(8,128)(2,1)} async-done(((bf16[264,264]{1,0:T(8,128)(2,1)}), bf16[2112,264]{1,0:T(8,128)(2,1)}) %all-gather.14.cloned.1.call-update) | async-done | bytes 1115152 | tf_op jit(solution)/shard_map/all_gather | solution.py:85
  377.1 45.3 %all-gather.20.cloned.1.call-done = bf16[2112,264]{1,0:T(8,128)(2,1)} async-done(((bf16[264,264]{1,0:T(8,128)(2,1)}), bf16[2112,264]{1,0:T(8,128)(2,1)}) %all-gather.20.cloned.1.call-update) | async-done | bytes 1115152 | tf_op jit(solution)/shard_map/all_gather | solution.py:88
  422.4 5.0 convolution_convert_fusion.1
  427.4 0.0 all-reduce.7.cloned.1.call-update
  427.4 0.2 all-reduce.9.cloned.1.call-start
  427.6 35.0 %all-reduce.7.cloned.1.call-done = bf16[256,2112]{0,1:T(8,128)(2,1)} async-done(((bf16[256,2112]{0,1:T(8,128)(2,1)}), bf16[256,2112]{0,1:T(8,128)(2,1)}) %all-reduce.7.cloned.1.call-update) | async-done | bytes 1081360 | tf_op jit(solution)/shard_map/psum | solution.py:20
  462.6 1.7 fusion.3
  464.3 1.8 fusion.16
  466.1 0.0 copy-done.1
  466.1 1.4 fusion.32
  467.5 6.6 %convolution_convert_fusion = bf16[256,2112]{0,1:T(8,128)(2,1)} fusion(bf16[2112,768]{1,0:T(8,128)(2,1)} %all-gather.12.cloned.1.call-done, bf16[2112,768]{1,0:T(8,128)(2,1)} %all-gather.10.cloned.1.call-done, f32[256,768]{1,0:T(8,128)S(1)} %fusion.32, bf16[256,2112]{0,1:T(8,128)(2,1)S(1)} %get-tuple-element.15, f32[2112]{0:T(1024)S(1)} %get-tuple-element.10, ...), kind=kOutput, calls=%fused_computation | convolution fusion | flops 1664827392 | bytes 9446656 | tf_op jit(solution)/shard_map/dot_general | solution.py:17
  474.1 0.0 all-reduce.9.cloned.1.call-update
  474.1 37.2 %all-reduce.9.cloned.1.call-done = bf16[256,2112]{0,1:T(8,128)(2,1)} async-done(((bf16[256,2112]{0,1:T(8,128)(2,1)}), bf16[256,2112]{0,1:T(8,128)(2,1)}) %all-reduce.9.cloned.1.call-update) | async-done | bytes 1081360 | tf_op jit(solution)/shard_map/psum | solution.py:20
  511.3 1.5 fusion.5
  512.9 2.7 fusion.19
  (9 shorter events, 0.1 us)
Async XLA Ops:
  6.5 66.8 %copy-start = (bf16[256,2112]{0,1:T(8,128)(2,1)S(1)}, bf16[256,2112]{0,1:T(8,128)(2,1)}, u32[]{:S(2)}) copy-start(bf16[256,2112]{0,1:T(8,128)(2,1)} %param.10) | copy-start | bytes 3244036
  6.5 66.8 %all-gather.8.cloned.1.call-start = ((), (), s32[]{:S(2)}) async-start(), calls=%async_computation | async-start | bytes 3649536 | tf_op jit(solution)/shard_map/all_gather | solution.py:78
  7.3 128.0 %all-gather.10.cloned.1.call-start = ((), (), s32[]{:S(2)}) async-start(), calls=%async_computation.1 | async-start | bytes 3649536 | tf_op jit(solution)/shard_map/all_gather | solution.py:79
  8.0 189.2 %all-gather.12.cloned.1.call-start = ((), (), s32[]{:S(2)}) async-start(), calls=%async_computation.2 | async-start | bytes 3649536 | tf_op jit(solution)/shard_map/all_gather | solution.py:80
  8.7 230.7 %all-reduce.5.cloned.1.call-start = ((), (), s32[]{:S(2)}) async-start(), calls=%async_computation.3 | async-start | bytes 2162688 | tf_op jit(solution)/shard_map/psum | solution.py:20
  203.9 82.7 %all-gather.16.cloned.1.call-start = ((), (), s32[]{:S(2)}) async-start(), calls=%async_computation.5 | async-start | bytes 1824768 | tf_op jit(solution)/shard_map/all_gather | solution.py:86
  204.5 127.3 %all-gather.18.cloned.1.call-start = ((), (), s32[]{:S(2)}) async-start(), calls=%async_computation.6 | async-start | bytes 1824768 | tf_op jit(solution)/shard_map/all_gather | solution.py:87
  205.0 172.0 %all-gather.14.cloned.1.call-start = ((), (), s32[]{:S(2)}) async-start(), calls=%async_computation.4 | async-start | bytes 1824768 | tf_op jit(solution)/shard_map/all_gather | solution.py:85
  205.8 216.6 %all-gather.20.cloned.1.call-start = ((), (), s32[]{:S(2)}) async-start(), calls=%async_computation.7 | async-start | bytes 1824768 | tf_op jit(solution)/shard_map/all_gather | solution.py:88
  206.5 256.0 %all-reduce.7.cloned.1.call-start = ((), (), s32[]{:S(2)}) async-start(), calls=%async_computation.8 | async-start | bytes 2162688 | tf_op jit(solution)/shard_map/psum | solution.py:20
  427.4 83.9 %all-reduce.9.cloned.1.call-start = ((), (), s32[]{:S(2)}) async-start(), calls=%async_computation.9 | async-start | bytes 2162688 | tf_op jit(solution)/shard_map/psum | solution.py:20
  462.6 3.6 copy-start.1
Sparse Core Ops, SparseCore 0:
  9.5 63.7 all-gather.7
  75.5 59.7 all-gather.9
  137.5 59.7 all-gather.11
  204.0 35.3 all-reduce.4
  241.4 45.0 all-gather.15
  288.6 43.0 all-gather.17
  333.9 43.0 all-gather.13
  379.3 43.0 all-gather.19
  427.5 35.0 all-reduce.6
  474.3 37.0 all-reduce.8
where the time goes:
time: 523 us; the launch traced here: 522 us
  waiting for transfers between devices  466 us (89%)
  matrix products  27.7 us (5%)
  other arithmetic  13.6 us (3%)
  between operations  13.6 us (3%)
    psum x3, waiting for transfers between devices, narrow(): lax.psum(partial_value.astype(jnp.bfloat16), 'tp').astype(jnp.float32)  104 us
    all_gather x1, waiting for transfers between devices, local(): lax.all_gather(down_proj, 'fs', axis=0, tiled=True)  62 us
    all_gather x1, waiting for transfers between devices, local(): lax.all_gather(gate_proj, 'fs', axis=0, tiled=True)  61.5 us
    all_gather x1, waiting for transfers between devices, local(): lax.all_gather(up_proj, 'fs', axis=0, tiled=True)  58.7 us
    all_gather x1, waiting for transfers between devices, local(): lax.all_gather(mixer_out, 'fs', axis=0, tiled=True)  45.3 us
    all_gather x1, waiting for transfers between devices, local(): lax.all_gather(inner_gate, 'fs', axis=0, tiled=True)  43.7 us
    all_gather x1, waiting for transfers between devices, local(): lax.all_gather(outer_gate, 'fs', axis=0, tiled=True)  42.9 us
    all_gather x1, waiting for transfers between devices, local(): lax.all_gather(value_proj, 'fs', axis=0, tiled=True)  42.7 us
  transfers between devices with their start and end apart: 10, of which 10 were waited for; matrix products, arithmetic and copies ran while one was open for 3% of the time, Pallas kernels for 0%

commit v1 on v0

v1 whole, which is shorter than its diff:
```python
import functools

import jax
import jax.numpy as jnp
from jax import lax
from jax.experimental import pallas as pl
from jax.experimental.pallas import tpu as pltpu
from jax.sharding import PartitionSpec as P

MESH = pl.DeviceIdType.MESH
EPSILON = 1e-06
CONV_K = 3
F32, BF16 = jnp.float32, jnp.bfloat16
NT = (((1,), (1,)), ((), ()))


def kernel(cfg, *refs):
    Z, Y, X, shard, width, hc, nff, main, rem = cfg
    own_refs = refs[: nff + 2]
    stream_ref, gains_ref, taps_ref, out_ref = refs[nff + 2 : nff + 6]
    (ff, g3, g4, normed, acc, hidden, csend, crecv, xsend, xrecv, res,
     lsem, zsend, recv, asend, arecv, csem, xssem, xrsem, rsem) = refs[nff + 6 :]
    rows, Dp = stream_ref.shape
    half = rows // 2
    K3, K4 = nff, nff + 1
    f, t = lax.axis_index("fs"), lax.axis_index("tp")
    z, y = f // Y, f % Y
    c, x = t % 2, t // 2
    core_peer = (f, x * 2 + 1 - c)
    x_peers = [(f, ((x + j) % X) * 2 + c) for j in range(1, X)]

    def dev_z(zz):
        return (zz * Y + y, t)

    dev_y = (z * Y + (Y - 1 - y), t)

    barrier = pltpu.get_barrier_semaphore()

    def greet(d):
        pl.semaphore_signal(barrier, inc=1, device_id=d, device_id_type=MESH)

    always = [core_peer] + x_peers + ([dev_y] if Y == 2 else [])
    for d in always:
        greet(d)
    if Z > 1:
        @pl.when(z > 0)
        def _():
            greet(dev_z(z - 1))

        @pl.when(z < Z - 1)
        def _():
            greet(dev_z(z + 1))

    def slot(k, first, count):
        at = pl.ds(pl.multiple_of(first * shard, 16), count * shard)
        if k < nff:
            return ff.at[k, at]
        return (g3 if k == K3 else g4).at[at]

    local = [
        pltpu.make_async_copy(own_refs[k], slot(k, f, 1), lsem.at[k]) for k in range(nff + 2)
    ]
    for copy in local:
        copy.start()

    peers = len(always)
    if Z > 1:
        peers = peers + (z > 0).astype(jnp.int32) + (z < Z - 1).astype(jnp.int32)
    pl.semaphore_wait(barrier, peers)

    def remote(k, s, way, d):
        ref = slot(k, s, 1)
        return pltpu.make_async_remote_copy(
            src_ref=ref, dst_ref=ref, send_sem=zsend.at[k, way, s], recv_sem=recv.at[k, s],
            device_id=d, device_id_type=MESH,
        )

    def remote_a(s, way, d):
        ref = slot(K4, s * Y, Y)
        return pltpu.make_async_remote_copy(
            src_ref=ref, dst_ref=ref, send_sem=asend.at[way, s], recv_sem=arecv.at[s],
            device_id=d, device_id_type=MESH,
        )

    def right(k, s, act):
        @pl.when(z < Z - 1)
        def _():
            act(remote(k, s * Y + y, 0, dev_z(z + 1)))

    def left(k, s, act):
        @pl.when(z > 0)
        def _():
            act(remote(k, s * Y + y, 1, dev_z(z - 1)))

    def across(k, s, act):
        if Y == 2:
            act(remote(k, s * Y + y, 2, dev_y))

    def go(copy):
        copy.start()

    def own(k):
        right(k, z, go)
        left(k, z, go)
        across(k, z, go)

    def zsteps(k):
        def step(i, carry):
            @pl.when(z - 1 - i >= 0)
            def _():
                s = z - 1 - i
                remote(k, s * Y + y, 0, dev_z(z - 1)).wait_recv()
                right(k, s, go)
                across(k, s, go)

            @pl.when(z + 1 + i < Z)
            def _():
                s = z + 1 + i
                remote(k, s * Y + y, 0, dev_z(z + 1)).wait_recv()
                left(k, s, go)
                across(k, s, go)

            return carry

        lax.fori_loop(0, Z - 1, step, 0)

    def wait_across(k):
        if Y == 2:
            def step(s, carry):
                remote(k, s * Y + 1 - y, 2, dev_y).wait_recv()
                return carry

            lax.fori_loop(0, Z, step, 0)

    def right_a(s, act):
        @pl.when(z < Z - 1)
        def _():
            act(remote_a(s, 0, dev_z(z + 1)))

    def left_a(s, act):
        @pl.when(z > 0)
        def _():
            act(remote_a(s, 1, dev_z(z - 1)))

    def start_a():
        if Y == 2:
            remote(K4, z * Y + 1 - y, 2, dev_y).wait_recv()
        right_a(z, go)
        left_a(z, go)

    def steps_a(forward):
        def step(i, carry):
            @pl.when((z - 1 - i >= 0) & ((z < Z - 1) if forward else (z == Z - 1)))
            def _():
                s = z - 1 - i
                remote_a(s, 0, dev_z(z - 1)).wait_recv()
                if forward:
                    right_a(s, go)

            @pl.when((z + 1 + i < Z) & ((z > 0) if forward else (z == 0)))
            def _():
                s = z + 1 + i
                remote_a(s, 0, dev_z(z + 1)).wait_recv()
                if forward:
                    left_a(s, go)

            return carry

        lax.fori_loop(0, Z - 1, step, 0)

    def scaled(values, row):
        mean = jnp.sum(values * values, axis=-1, keepdims=True) * (1.0 / width)
        return values * lax.rsqrt(mean + EPSILON) * gains_ref[row : row + 1, :]

    def norm_to(source, row):
        def block(i, carry):
            at = pl.ds(pl.multiple_of(i * 32, 32), 32)
            normed[at] = scaled(source[at].astype(F32), row).astype(BF16)
            return carry

        lax.fori_loop(0, rows // 32, block, 0)

    def ffn_chunk(k, first):
        weights = ff.at[k]

        def block(i, carry):
            at = pl.ds(pl.multiple_of(i * half, 16), half)
            n = normed[at]
            gate = jnp.dot(n, weights[:, 0:hc], preferred_element_type=F32)
            up = jnp.dot(n, weights[:, hc : 2 * hc], preferred_element_type=F32)
            h = (gate / (1.0 + jnp.exp(-gate)) * up).astype(BF16)
            part = lax.dot_general(h, weights[:, 2 * hc :], NT, preferred_element_type=F32)
            acc[at] = part if first else acc[at] + part
            return carry

        lax.fori_loop(0, 2, block, 0)

    mine = pl.ds(pl.multiple_of(c * half, 16), half)
    other = pl.ds(pl.multiple_of((1 - c) * half, 16), half)

    def reduce(r, source, row, factor):
        csend[r] = acc[other].astype(BF16)
        first = pltpu.make_async_remote_copy(
            src_ref=csend.at[r], dst_ref=crecv.at[r], send_sem=csem.at[0, r],
            recv_sem=csem.at[1, r], device_id=core_peer, device_id_type=MESH,
        )
        first.start()
        first.wait()
        xsend[r] = (acc[mine].astype(BF16).astype(F32) + crecv[r].astype(F32)).astype(BF16)
        sends = []
        for j, peer in enumerate(x_peers):
            copy = pltpu.make_async_remote_copy(
                src_ref=xsend.at[r], dst_ref=xrecv.at[r, j], send_sem=xssem.at[r, j],
                recv_sem=xrsem.at[r, j], device_id=peer, device_id_type=MESH,
            )
            copy.start()
            sends.append(copy)
        for copy in sends:
            copy.wait()

        def block(i, carry):
            at = pl.ds(pl.multiple_of(i * 32, 16), 32)
            full = pl.ds(pl.multiple_of(c * half + i * 32, 16), 32)
            total = xsend[r, at].astype(F32)
            for j in range(X - 1):
                total = total + xrecv[r, j, at].astype(F32)
            res[r, full] = (
                source[full].astype(F32) + factor * scaled(total, row)
            ).astype(BF16)
            return carry

        lax.fori_loop(0, half // 32, block, 0)
        last = pltpu.make_async_remote_copy(
            src_ref=res.at[r, mine], dst_ref=res.at[r, mine], send_sem=rsem.at[0, r],
            recv_sem=rsem.at[1, r], device_id=core_peer, device_id_type=MESH,
        )
        last.start()
        last.wait_send()
        pltpu.make_async_remote_copy(
            src_ref=res.at[r, other], dst_ref=res.at[r, other], send_sem=rsem.at[0, r],
            recv_sem=rsem.at[1, r], device_id=core_peer, device_id_type=MESH,
        ).wait_recv()

    def mixer():
        edge = main + 128
        outer_inner = jnp.dot(normed[...], g3[...], preferred_element_type=F32)
        outer_inner = outer_inner.astype(BF16).astype(F32)
        value_rest = jnp.dot(normed[...], g4[:, 0:edge], preferred_element_type=F32)
        value_rest = value_rest.astype(BF16).astype(F32)
        rest = value_rest[:, main:]
        if rem:
            lane = lax.broadcasted_iota(jnp.int32, rest.shape, 1)
            keep = (lane >= 3 * rem) & (lane < 4 * rem)
            rests = [
                jnp.where(keep, pltpu.roll(rest, (3 - j) * rem, 1), 0.0) for j in range(3)
            ]
        else:
            rests = [jnp.zeros_like(rest)] * 3
        outer = jnp.concatenate([rests[0], outer_inner[:, 0:main]], axis=1)
        inner = jnp.concatenate([rests[1], outer_inner[:, main:]], axis=1)
        value = jnp.concatenate([rests[2], value_rest[:, 0:main]], axis=1)
        gated = inner * value
        token = lax.broadcasted_iota(jnp.int32, gated.shape, 0)
        conv = jnp.zeros_like(gated)
        for j in range(CONV_K):
            back = CONV_K - 1 - j
            moved = gated
            if back:
                moved = jnp.where(token >= back, pltpu.roll(gated, back, 0), 0.0)
            conv = conv + taps_ref[j : j + 1, :] * moved
        hidden[...] = (outer * conv).astype(BF16)

        def block(i, carry):
            at = pl.ds(pl.multiple_of(i * half, 16), half)
            acc[at] = lax.dot_general(
                hidden[at], g4[:, main:], NT, preferred_element_type=F32
            )
            return carry

        lax.fori_loop(0, 2, block, 0)

    for k, copy in enumerate(local):
        copy.wait()
        if k < 2:
            own(k)
    norm_to(stream_ref, 0)
    for k in range(nff):
        zsteps(k)
        if k + 2 <= K3:
            own(k + 2)
        if k + 2 == K3:
            across(K4, z, go)
        if k > 0:
            wait_across(k - 1)
            ffn_chunk(k - 1, k == 1)
    zsteps(K3)
    start_a()
    steps_a(True)
    wait_across(nff - 1)
    ffn_chunk(nff - 1, nff == 1)
    reduce(0, stream_ref, 1, 0.5)
    norm_to(res.at[0], 2)
    wait_across(K3)
    steps_a(False)
    mixer()
    reduce(1, res.at[0], 3, 1.0)
    norm_to(res.at[1], 4)
    acc[...] = jnp.zeros_like(acc)

    def again(k, carry):
        ffn_chunk(k, False)
        return carry

    lax.fori_loop(0, nff, again, 0)
    reduce(2, res.at[1], 5, 0.5)
    out_ref[...] = res[2]

    def done(copy):
        copy.wait_send()

    for k in range(nff + 1):
        def drain(s, carry):
            @pl.when(s <= z)
            def _():
                right(k, s, done)

            @pl.when(s >= z)
            def _():
                left(k, s, done)

            across(k, s, done)
            return carry

        lax.fori_loop(0, Z, drain, 0)
    across(K4, z, done)

    def drain_a(s, carry):
        @pl.when(s <= z)
        def _():
            right_a(s, done)

        @pl.when(s >= z)
        def _():
            left_a(s, done)

        return carry

    lax.fori_loop(0, Z, drain_a, 0)


def y_count(mesh):
    try:
        found = len({d.coords[1] for d in mesh.devices.reshape(-1)})
    except AttributeError:
        found = 1
    return found if found == 2 and mesh.shape["fs"] % 2 == 0 else 1


def solution(mesh):
    n_fs, n_tp = mesh.shape["fs"], mesh.shape["tp"]
    Y = y_count(mesh)
    Z, X = n_fs // Y, n_tp // 2

    def local(stream_in, norm_gains, gate, up, down, outer_w, inner_w, value_w, mixer_w, conv_taps):
        rows, width = stream_in.shape
        part, hid = gate.shape
        channels = outer_w.shape[1]
        shard = -(-part // 16) * 16
        Dp = n_fs * shard
        nff = 3 if hid % 384 == 0 else 1
        hc = hid // nff
        main = channels // 128 * 128
        rem = channels - main

        def widen(v):
            lead = v.shape[0]
            v = v.reshape(lead, n_fs, part)
            return jnp.pad(v, ((0, 0), (0, 0), (0, shard - part))).reshape(lead, Dp)

        def pack(parts):
            w = jnp.concatenate(parts, axis=1)
            return jnp.pad(w, ((0, shard - part), (0, 0)))

        owns = [
            pack([w[:, k * hc : (k + 1) * hc] for w in (gate, up, down)]) for k in range(nff)
        ]
        owns.append(pack([outer_w[:, :main], inner_w[:, :main]]))
        rest = [w[:, main:] for w in (outer_w, inner_w, value_w, mixer_w)]
        rest.append(jnp.zeros((part, 128 - 4 * rem), BF16))
        owns.append(pack([value_w[:, :main]] + rest + [mixer_w[:, :main]]))
        taps = lax.dynamic_slice_in_dim(
            conv_taps, lax.axis_index("tp") * channels, channels, 1
        ).astype(F32)
        taps = jnp.concatenate(
            [jnp.pad(taps[:, main:], ((0, 0), (3 * rem, 128 - 4 * rem))), taps[:, :main]], axis=1
        )
        half = rows // 2
        dma, vmem = pltpu.SemaphoreType.DMA, pltpu.VMEM
        out = pl.pallas_call(
            functools.partial(kernel, (Z, Y, X, shard, width, hc, nff, main, rem)),
            out_shape=jax.ShapeDtypeStruct((rows, Dp), BF16),
            in_specs=[pl.BlockSpec(memory_space=pl.ANY)] * (nff + 2)
            + [pl.BlockSpec(memory_space=pltpu.VMEM)] * 3,
            out_specs=pl.BlockSpec(memory_space=pltpu.VMEM),
            scratch_shapes=[
                vmem((nff, Dp, 3 * hc), BF16),
                vmem((Dp, 2 * main), BF16),
                vmem((Dp, 2 * main + 128), BF16),
                vmem((rows, Dp), BF16),
                vmem((rows, Dp), F32),
                vmem((rows, main + 128), BF16),
                vmem((3, half, Dp), BF16),
                vmem((3, half, Dp), BF16),
                vmem((3, half, Dp), BF16),
                vmem((3, X - 1, half, Dp), BF16),
                vmem((3, rows, Dp), BF16),
                dma((nff + 2,)),
                dma((nff + 2, 3, n_fs)),
                dma((nff + 2, n_fs)),
                dma((2, Z)),
                dma((Z,)),
                dma((2, 3)),
                dma((3, X - 1)),
                dma((3, X - 1)),
                dma((2, 3)),
            ],
            compiler_params=pltpu.CompilerParams(
                collective_id=0, has_side_effects=True, vmem_limit_bytes=60 * 1024 * 1024
            ),
        )(*owns, widen(stream_in), widen(norm_gains), taps)
        return out.reshape(rows, n_fs, shard)[:, :, :part].reshape(rows, width)

    return jax.shard_map(
        local,
        mesh=mesh,
        in_specs=(P("fs", None), P()) + (P("fs", "tp"),) * 7 + (P(),),
        out_specs=P("fs", None),
        check_vma=False,
    )
```

time: 523 us -> 216 us (0.41)
  waiting for transfers between devices: 466 us -> 0 us
  Pallas kernels: 0 us -> 204 us
  matrix products: 27.7 us -> 0 us
  between operations: 13.6 us -> 0.16 us
  other arithmetic: 13.6 us -> 3.96 us
  local copies, waits for them, and re-layouts: 1.48 us -> 7.53 us
    all_gather x7 -> x0, waiting for transfers between devices: 357 us -> none  [the longest x1 62 us: local(): lax.all_gather(down_proj, 'fs', axis=0, tiled=True)]
    pallas_call x0 -> x1, Pallas kernels: none -> 204 us  [local(): pl.pallas_call(functools.partial(kernel, (Z, Y, X, shard, width, hc, nff,...]
    psum x3 -> x0, waiting for transfers between devices: 104 us -> none  [narrow(): lax.psum(partial_value.astype(jnp.bfloat16), 'tp').astype(jnp.float32)]
    dot_general x7 -> x0, matrix products: 27.7 us -> none  [the longest x3 18.2 us: narrow(): lax.dot_general(inner, weight, (((1,), (1,)), ((), ())), preferred_elemen...]
    reduce_sum x6 -> x0, other arithmetic: 10.1 us -> none  [scaled(): jnp.mean(values * values, axis=-1, keepdims=True) + EPSILON]
  transfers between devices with their start and end apart: 10 -> 0, of which waited for: 10 -> 0; matrix products, arithmetic and copies ran while one was open for 3% -> 0% of each run, Pallas kernels for 0% -> 0%
where the time goes in v1:
time: 216 us; the launch traced here: 215 us
  Pallas kernels  204 us (94%)
  local copies, waits for them, and re-layouts  7.53 us (3%)
  other arithmetic  3.96 us (2%)
    pallas_call x1, Pallas kernels, local(): pl.pallas_call(functools.partial(kernel, (Z, Y, X, shard, width, hc, nff,...  204 us

profile of v1, /device:TPU:0, one launch (start us, length us, event | category | flops | bytes accessed | tf_op | source)
XLA Modules:
  0.0 215.4 jit_solution(11498743777023783377)
XLA Ops:
  0.0 0.0 slice-start.3
  0.0 0.0 slice-start.1
  0.0 0.8 dynamic-slice_convert_fusion
  0.8 0.7 select_maximum_fusion.refs_7_
  1.5 0.0 slice-start
  1.5 0.0 slice-start.2
  1.5 0.0 slice-start.4
  1.5 0.0 slice-start.5
  1.5 0.0 slice-start.6
  1.5 0.0 slice-start.7
  1.5 1.0 reshape.20
  2.6 0.7 reshape.21.refs_6_
  3.3 0.0 slice-done.3
  3.3 0.0 slice-done.1
  3.3 0.7 fusion.17.refs_3_
  4.0 0.0 copy-start.1
  4.1 0.0 slice-done
  4.1 0.0 slice-done.2
  4.1 0.0 slice-done.4
  4.1 0.0 slice-done.5
  4.1 0.0 slice-done.6
  4.1 0.0 slice-done.7
  4.1 0.0 copy-start.2
  4.1 0.2 concatenate.22
  4.3 0.0 copy-start.3
  4.4 0.8 pad.34.refs_4_
  5.1 0.0 copy-done.1
  5.2 0.0 copy-done.2
  5.2 0.3 copy-done.3
  5.6 0.0 copy-start
  5.6 0.8 fusion.16.refs_2_
  6.4 1.0 fusion.12
  7.3 0.0 copy-done
  7.3 0.1 pad.35
  7.4 1.5 copy.13.refs_5_
  8.9 203.8 %shard_map.100 = bf16[256,2176]{1,0:T(8,128)(2,1)} custom-call(bf16[272,768]{1,0:T(8,128)(2,1)} %get-tuple-element.14.refs_0_, bf16[272,768]{1,0:T(8,128)(2,1)} %get-tuple-element.15.refs_1_, bf16[272,768]{1,0:T(8,128)(2,1)} %fusion.16.refs_2_, bf16[272,512]{1,0:T(8,128)(2,1)} %fusion.17.refs_3_, bf16[272,640]{1,0:T(8,128)(2,1)} %pad.34.refs_4_, ...), custom_call_target="tpu_custom_call" | custom-call | tf_op jit(solution)/shard_map/pallas_call | solution.py:399
  212.7 1.7 copy.14
  214.4 1.1 slice.82
  (7 shorter events, 0.1 us)
Async XLA Ops:
  0.0 3.3 %slice-start.3 = ((bf16[264,264]{1,0:T(8,128)(2,1)}), bf16[264,256]{1,0:T(8,128)(2,1)S(1)}, s32[]{:S(2)}) async-start(bf16[264,264]{1,0:T(8,128)(2,1)} %param.16), calls=%async_computation.3 | async-start | bytes 270336 | tf_op jit(solution)/shard_map/slice | solution.py:387
  0.0 3.3 %slice-start.1 = ((bf16[264,264]{1,0:T(8,128)(2,1)}), bf16[264,256]{1,0:T(8,128)(2,1)S(1)}, s32[]{:S(2)}) async-start(bf16[264,264]{1,0:T(8,128)(2,1)} %param.15), calls=%async_computation.1 | async-start | bytes 270336 | tf_op jit(solution)/shard_map/slice | solution.py:387
  1.5 2.6 %slice-start = ((bf16[264,264]{1,0:T(8,128)(2,1)}), bf16[264,8]{1,0:T(8,128)(2,1)S(1)}, s32[]{:S(2)}) async-start(bf16[264,264]{1,0:T(8,128)(2,1)} %param.15), calls=%async_computation | async-start | bytes 135168 | tf_op jit(solution)/shard_map/slice | solution.py:388
  1.5 2.6 %slice-start.2 = ((bf16[264,264]{1,0:T(8,128)(2,1)}), bf16[264,8]{1,0:T(8,128)(2,1)S(1)}, s32[]{:S(2)}) async-start(bf16[264,264]{1,0:T(8,128)(2,1)} %param.16), calls=%async_computation.2 | async-start | bytes 135168 | tf_op jit(solution)/shard_map/slice | solution.py:388
  1.5 2.6 %slice-start.4 = ((bf16[264,264]{1,0:T(8,128)(2,1)}), bf16[264,8]{1,0:T(8,128)(2,1)S(1)}, s32[]{:S(2)}) async-start(bf16[264,264]{1,0:T(8,128)(2,1)} %param.17), calls=%async_computation.4 | async-start | bytes 135168 | tf_op jit(solution)/shard_map/slice | solution.py:388
  1.5 2.6 %slice-start.5 = ((bf16[264,264]{1,0:T(8,128)(2,1)}), bf16[264,256]{1,0:T(8,128)(2,1)S(1)}, s32[]{:S(2)}) async-start(bf16[264,264]{1,0:T(8,128)(2,1)} %param.17), calls=%async_computation.5 | async-start | bytes 270336 | tf_op jit(solution)/shard_map/slice | solution.py:390
  1.5 2.6 %slice-start.6 = ((bf16[264,264]{1,0:T(8,128)(2,1)}), bf16[264,8]{1,0:T(8,128)(2,1)S(1)}, s32[]{:S(2)}) async-start(bf16[264,264]{1,0:T(8,128)(2,1)} %param.18), calls=%async_computation.6 | async-start | bytes 135168 | tf_op jit(solution)/shard_map/slice | solution.py:388
  1.5 2.6 %slice-start.7 = ((bf16[264,264]{1,0:T(8,128)(2,1)}), bf16[264,256]{1,0:T(8,128)(2,1)S(1)}, s32[]{:S(2)}) async-start(bf16[264,264]{1,0:T(8,128)(2,1)} %param.18), calls=%async_computation.7 | async-start | bytes 270336 | tf_op jit(solution)/shard_map/slice | solution.py:390
  4.0 1.1 copy-start.1
  4.1 1.1 copy-start.2
  4.3 1.2 copy-start.3
  5.6 1.8 copy-start

commit v2 on v1

--- a/solution.py
+++ b/solution.py
@@ -15,13 +15,13 @@
 
 
 def kernel(cfg, *refs):
-    Z, Y, X, shard, width, hc, nff, main, rem = cfg
-    own_refs = refs[: nff + 2]
-    stream_ref, gains_ref, taps_ref, out_ref = refs[nff + 2 : nff + 6]
+    Z, Y, X, shard, sent, width, hc, nff, main, rem = cfg
+    own_refs = refs[:8]
+    stream_ref, gains_ref, taps_ref, out_ref = refs[8:12]
     (ff, g3, g4, normed, acc, hidden, csend, crecv, xsend, xrecv, res,
-     lsem, zsend, recv, asend, arecv, csem, xssem, xrsem, rsem) = refs[nff + 6 :]
+     lsem, zsend, recv, asend, arecv, csem, xssem, xrsem, rsem) = refs[12:]
     rows, Dp = stream_ref.shape
-    half = rows // 2
+    half, quarter = rows // 2, rows // 4
     K3, K4 = nff, nff + 1
     f, t = lax.axis_index("fs"), lax.axis_index("tp")
     z, y = f // Y, f % Y
@@ -34,6 +34,13 @@
 
     dev_y = (z * Y + (Y - 1 - y), t)
 
+    for s in range(Z * Y):
+        tail = pl.ds(s * shard + shard - 16, 16)
+        for k in range(nff):
+            ff[k, tail] = jnp.zeros((16, 3 * hc), BF16)
+        g3[tail] = jnp.zeros((16, 2 * main), BF16)
+        g4[tail] = jnp.zeros((16, 2 * main + 128), BF16)
+
     barrier = pltpu.get_barrier_semaphore()
 
     def greet(d):
@@ -52,15 +59,28 @@
             greet(dev_z(z + 1))
 
     def slot(k, first, count):
-        at = pl.ds(pl.multiple_of(first * shard, 16), count * shard)
+        at = pl.ds(pl.multiple_of(first * shard, 16), (count - 1) * shard + sent)
         if k < nff:
             return ff.at[k, at]
         return (g3 if k == K3 else g4).at[at]
 
+    here = pl.ds(pl.multiple_of(f * shard, 16), sent)
+    moves = []
+    for k in range(nff):
+        for j in range(3):
+            moves.append((k, own_refs[j].at[:, pl.ds(k * hc, hc)],
+                          ff.at[k, here, pl.ds(j * hc, hc)]))
+    ow, iw, vw, mw, rw = own_refs[3:]
+    lead = pl.ds(0, main)
+    moves.append((K3, ow.at[:, lead], g3.at[here, lead]))
+    moves.append((K3, iw.at[:, lead], g3.at[here, pl.ds(main, main)]))
+    moves.append((K4, vw.at[:, lead], g4.at[here, lead]))
+    moves.append((K4, rw, g4.at[here, pl.ds(main, 128)]))
+    moves.append((K4, mw.at[:, lead], g4.at[here, pl.ds(main + 128, main)]))
     local = [
-        pltpu.make_async_copy(own_refs[k], slot(k, f, 1), lsem.at[k]) for k in range(nff + 2)
+        (k, pltpu.make_async_copy(src, dst, lsem.at[n])) for n, (k, src, dst) in enumerate(moves)
     ]
-    for copy in local:
+    for _, copy in local:
         copy.start()
 
     peers = len(always)
@@ -175,77 +195,103 @@
     def norm_to(source, row):
         def block(i, carry):
             at = pl.ds(pl.multiple_of(i * 32, 32), 32)
-            normed[at] = scaled(source[at].astype(F32), row).astype(BF16)
+            per_half, per_quarter = half // 32, quarter // 32
+            h, b = i // per_half, (i % per_half) // per_quarter
+            to = pl.ds(pl.multiple_of(h * quarter + (i % per_quarter) * 32, 32), 32)
+            normed[b, to] = scaled(source[at].astype(F32), row).astype(BF16)
             return carry
 
         lax.fori_loop(0, rows // 32, block, 0)
 
+    def ffn_block(k, b, first):
+        weights = ff.at[k]
+        n = normed[b]
+        gate = jnp.dot(n, weights[:, 0:hc], preferred_element_type=F32)
+        up = jnp.dot(n, weights[:, hc : 2 * hc], preferred_element_type=F32)
+        h = (gate / (1.0 + jnp.exp(-gate)) * up).astype(BF16)
+        part = lax.dot_general(h, weights[:, 2 * hc :], NT, preferred_element_type=F32)
+        acc[b] = part if first else acc[b] + part
+
     def ffn_chunk(k, first):
-        weights = ff.at[k]
-
-        def block(i, carry):
-            at = pl.ds(pl.multiple_of(i * half, 16), half)
-            n = normed[at]
-            gate = jnp.dot(n, weights[:, 0:hc], preferred_element_type=F32)
-            up = jnp.dot(n, weights[:, hc : 2 * hc], preferred_element_type=F32)
-            h = (gate / (1.0 + jnp.exp(-gate)) * up).astype(BF16)
-            part = lax.dot_general(h, weights[:, 2 * hc :], NT, preferred_element_type=F32)
-            acc[at] = part if first else acc[at] + part
+        def block(b, carry):
+            ffn_block(k, b, first)
             return carry
 
         lax.fori_loop(0, 2, block, 0)
 
-    mine = pl.ds(pl.multiple_of(c * half, 16), half)
-    other = pl.ds(pl.multiple_of((1 - c) * half, 16), half)
-
-    def reduce(r, source, row, factor):
-        csend[r] = acc[other].astype(BF16)
-        first = pltpu.make_async_remote_copy(
-            src_ref=csend.at[r], dst_ref=crecv.at[r], send_sem=csem.at[0, r],
-            recv_sem=csem.at[1, r], device_id=core_peer, device_id_type=MESH,
-        )
-        first.start()
-        first.wait()
-        xsend[r] = (acc[mine].astype(BF16).astype(F32) + crecv[r].astype(F32)).astype(BF16)
-        sends = []
-        for j, peer in enumerate(x_peers):
-            copy = pltpu.make_async_remote_copy(
-                src_ref=xsend.at[r], dst_ref=xrecv.at[r, j], send_sem=xssem.at[r, j],
-                recv_sem=xrsem.at[r, j], device_id=peer, device_id_type=MESH,
-            )
-            copy.start()
-            sends.append(copy)
-        for copy in sends:
-            copy.wait()
-
-        def block(i, carry):
-            at = pl.ds(pl.multiple_of(i * 32, 16), 32)
-            full = pl.ds(pl.multiple_of(c * half + i * 32, 16), 32)
-            total = xsend[r, at].astype(F32)
+    mine = pl.ds(pl.multiple_of(c * quarter, 16), quarter)
+    other = pl.ds(pl.multiple_of((1 - c) * quarter, 16), quarter)
+
+    def core_copy(r, b):
+        return pltpu.make_async_remote_copy(
+            src_ref=csend.at[r, b], dst_ref=crecv.at[r, b], send_sem=csem.at[0, r, b],
+            recv_sem=csem.at[1, r, b], device_id=core_peer, device_id_type=MESH,
+        )
+
+    def x_copy(r, b, j):
+        return pltpu.make_async_remote_copy(
+            src_ref=xsend.at[r, b], dst_ref=xrecv.at[r, b, j], send_sem=xssem.at[r, b, j],
+            recv_sem=xrsem.at[r, b, j], device_id=x_peers[j], device_id_type=MESH,
+        )
+
+    def res_copy(r, b, core):
+        at = pl.ds(pl.multiple_of(core * half + b * quarter, 16), quarter)
+        return pltpu.make_async_remote_copy(
+            src_ref=res.at[r, at], dst_ref=res.at[r, at], send_sem=rsem.at[0, r, b],
+            recv_sem=rsem.at[1, r, b], device_id=core_peer, device_id_type=MESH,
+        )
+
+    def reduce(r, compute, source, row, factor):
+        def send(b, carry):
+            compute(b)
+            csend[r, b] = acc[b, other].astype(BF16)
+            core_copy(r, b).start()
+            core_copy(r, b).wait()
+            xsend[r, b] = (
+                acc[b, mine].astype(BF16).astype(F32) + crecv[r, b].astype(F32)
+            ).astype(BF16)
             for j in range(X - 1):
-                total = total + xrecv[r, j, at].astype(F32)
-            res[r, full] = (
-                source[full].astype(F32) + factor * scaled(total, row)
-            ).astype(BF16)
-            return carry
-
-        lax.fori_loop(0, half // 32, block, 0)
-        last = pltpu.make_async_remote_copy(
-            src_ref=res.at[r, mine], dst_ref=res.at[r, mine], send_sem=rsem.at[0, r],
-            recv_sem=rsem.at[1, r], device_id=core_peer, device_id_type=MESH,
-        )
-        last.start()
-        last.wait_send()
-        pltpu.make_async_remote_copy(
-            src_ref=res.at[r, other], dst_ref=res.at[r, other], send_sem=rsem.at[0, r],
-            recv_sem=rsem.at[1, r], device_id=core_peer, device_id_type=MESH,
-        ).wait_recv()
+                x_copy(r, b, j).start()
+            return carry
+
+        def receive(b, carry):
+            for j in range(X - 1):
+                x_copy(r, b, j).wait()
+
+            def block(i, inner_carry):
+                at = pl.ds(pl.multiple_of(i * 32, 16), 32)
+                full = pl.ds(pl.multiple_of(c * half + b * quarter + i * 32, 16), 32)
+                total = xsend[r, b, at].astype(F32)
+                for j in range(X - 1):
+                    total = total + xrecv[r, b, j, at].astype(F32)
+                res[r, full] = (
+                    source[full].astype(F32) + factor * scaled(total, row)
+                ).astype(BF16)
+                return inner_carry
+
+            lax.fori_loop(0, quarter // 32, block, 0)
+            res_copy(r, b, c).start()
+            return carry
+
+        def finish(b, carry):
+            res_copy(r, b, c).wait_send()
+            res_copy(r, b, 1 - c).wait_recv()
+            return carry
+
+        lax.fori_loop(0, 2, send, 0)
+        lax.fori_loop(0, 2, receive, 0)
+        lax.fori_loop(0, 2, finish, 0)
+
+    def swapped(v):
+        q = [v[j * quarter : (j + 1) * quarter] for j in range(4)]
+        return jnp.concatenate([q[0], q[2], q[1], q[3]], axis=0)
 
     def mixer():
         edge = main + 128
-        outer_inner = jnp.dot(normed[...], g3[...], preferred_element_type=F32)
+        n = swapped(normed[...].reshape(rows, Dp))
+        outer_inner = jnp.dot(n, g3[...], preferred_element_type=F32)
         outer_inner = outer_inner.astype(BF16).astype(F32)
-        value_rest = jnp.dot(normed[...], g4[:, 0:edge], preferred_element_type=F32)
+        value_rest = jnp.dot(n, g4[:, 0:edge], preferred_element_type=F32)
         value_rest = value_rest.astype(BF16).astype(F32)
         rest = value_rest[:, main:]
         if rem:
@@ -268,19 +314,27 @@
             if back:
                 moved = jnp.where(token >= back, pltpu.roll(gated, back, 0), 0.0)
             conv = conv + taps_ref[j : j + 1, :] * moved
-        hidden[...] = (outer * conv).astype(BF16)
-
-        def block(i, carry):
-            at = pl.ds(pl.multiple_of(i * half, 16), half)
-            acc[at] = lax.dot_general(
-                hidden[at], g4[:, main:], NT, preferred_element_type=F32
-            )
-            return carry
-
-        lax.fori_loop(0, 2, block, 0)
-
-    for k, copy in enumerate(local):
-        copy.wait()
+        hidden[...] = swapped((outer * conv).astype(BF16)).reshape(hidden.shape)
+
+    def mixer_block(b):
+        acc[b] = lax.dot_general(hidden[b], g4[:, main:], NT, preferred_element_type=F32)
+
+    def last_chunk(b):
+        ffn_block(nff - 1, b, nff == 1)
+
+    def second(b):
+        acc[b] = jnp.zeros(acc.shape[1:], F32)
+
+        def again(k, carry):
+            ffn_block(k, b, False)
+            return carry
+
+        lax.fori_loop(0, nff, again, 0)
+
+    for k in range(nff + 2):
+        for owner, copy in local:
+            if owner == k:
+                copy.wait()
         if k < 2:
             own(k)
     norm_to(stream_ref, 0)
@@ -297,22 +351,14 @@
     start_a()
     steps_a(True)
     wait_across(nff - 1)
-    ffn_chunk(nff - 1, nff == 1)
-    reduce(0, stream_ref, 1, 0.5)
+    reduce(0, last_chunk, stream_ref, 1, 0.5)
     norm_to(res.at[0], 2)
     wait_across(K3)
     steps_a(False)
     mixer()
-    reduce(1, res.at[0], 3, 1.0)
+    reduce(1, mixer_block, res.at[0], 3, 1.0)
     norm_to(res.at[1], 4)
-    acc[...] = jnp.zeros_like(acc)
-
-    def again(k, carry):
-        ffn_chunk(k, False)
-        return carry
-
-    lax.fori_loop(0, nff, again, 0)
-    reduce(2, res.at[1], 5, 0.5)
+    reduce(2, second, res.at[1], 5, 0.5)
     out_ref[...] = res[2]
 
     def done(copy):
@@ -377,52 +423,50 @@
             v = v.reshape(lead, n_fs, part)
             return jnp.pad(v, ((0, 0), (0, 0), (0, shard - part))).reshape(lead, Dp)
 
-        def pack(parts):
-            w = jnp.concatenate(parts, axis=1)
-            return jnp.pad(w, ((0, shard - part), (0, 0)))
-
-        owns = [
-            pack([w[:, k * hc : (k + 1) * hc] for w in (gate, up, down)]) for k in range(nff)
-        ]
-        owns.append(pack([outer_w[:, :main], inner_w[:, :main]]))
+        sent = -(-part // 8) * 8
+
+        def pack(w):
+            return w if sent == part else jnp.pad(w, ((0, sent - part), (0, 0)))
+
         rest = [w[:, main:] for w in (outer_w, inner_w, value_w, mixer_w)]
         rest.append(jnp.zeros((part, 128 - 4 * rem), BF16))
-        owns.append(pack([value_w[:, :main]] + rest + [mixer_w[:, :main]]))
+        owns = [gate, up, down, outer_w, inner_w, value_w, mixer_w]
+        owns = [pack(w) for w in owns + [jnp.concatenate(rest, axis=1)]]
         taps = lax.dynamic_slice_in_dim(
             conv_taps, lax.axis_index("tp") * channels, channels, 1
         ).astype(F32)
         taps = jnp.concatenate(
             [jnp.pad(taps[:, main:], ((0, 0), (3 * rem, 128 - 4 * rem))), taps[:, :main]], axis=1
         )
-        half = rows // 2
+        half, quarter = rows // 2, rows // 4
         dma, vmem = pltpu.SemaphoreType.DMA, pltpu.VMEM
         out = pl.pallas_call(
-            functools.partial(kernel, (Z, Y, X, shard, width, hc, nff, main, rem)),
+            functools.partial(kernel, (Z, Y, X, shard, sent, width, hc, nff, main, rem)),
             out_shape=jax.ShapeDtypeStruct((rows, Dp), BF16),
-            in_specs=[pl.BlockSpec(memory_space=pl.ANY)] * (nff + 2)
+            in_specs=[pl.BlockSpec(memory_space=pl.ANY)] * 8
             + [pl.BlockSpec(memory_space=pltpu.VMEM)] * 3,
             out_specs=pl.BlockSpec(memory_space=pltpu.VMEM),
             scratch_shapes=[
                 vmem((nff, Dp, 3 * hc), BF16),
                 vmem((Dp, 2 * main), BF16),
                 vmem((Dp, 2 * main + 128), BF16),
-                vmem((rows, Dp), BF16),
-                vmem((rows, Dp), F32),
-                vmem((rows, main + 128), BF16),
-                vmem((3, half, Dp), BF16),
-                vmem((3, half, Dp), BF16),
-                vmem((3, half, Dp), BF16),
-                vmem((3, X - 1, half, Dp), BF16),
+                vmem((2, half, Dp), BF16),
+                vmem((2, half, Dp), F32),
+                vmem((2, half, main + 128), BF16),
+                vmem((3, 2, quarter, Dp), BF16),
+                vmem((3, 2, quarter, Dp), BF16),
+                vmem((3, 2, quarter, Dp), BF16),
+                vmem((3, 2, X - 1, quarter, Dp), BF16),
                 vmem((3, rows, Dp), BF16),
-                dma((nff + 2,)),
+                dma((3 * nff + 5,)),
                 dma((nff + 2, 3, n_fs)),
                 dma((nff + 2, n_fs)),
                 dma((2, Z)),
                 dma((Z,)),
-                dma((2, 3)),
-                dma((3, X - 1)),
-                dma((3, X - 1)),
-                dma((2, 3)),
+                dma((2, 3, 2)),
+                dma((3, 2, X - 1)),
+                dma((3, 2, X - 1)),
+                dma((2, 3, 2)),
             ],
             compiler_params=pltpu.CompilerParams(
                 collective_id=0, has_side_effects=True, vmem_limit_bytes=60 * 1024 * 1024

time: 216 us -> 205 us (0.949)
  Pallas kernels: 204 us -> 193 us
  local copies, waits for them, and re-layouts: 7.53 us -> 10.4 us
  other arithmetic: 3.96 us -> 1.52 us
    pallas_call x1, Pallas kernels: 204 us -> 193 us  [local(): pl.pallas_call(functools.partial(kernel, (Z, Y, X, shard, sent, width, hc...]
    slice x8 -> x4, local copies, waits for them, and re-layouts: 0.02 us -> 3.55 us  [local(): rest = [w[:, main:] for w in (outer_w, inner_w, value_w, mixer_w)]]
    concatenate x3 -> x0, other arithmetic: 2.48 us -> none  [pack(): w = jnp.concatenate(parts, axis=1)]
where the time goes in v2:
time: 205 us; the launch traced here: 204 us
  Pallas kernels  193 us (94%)
  local copies, waits for them, and re-layouts  10.4 us (5%)
    pallas_call x1, Pallas kernels, local(): pl.pallas_call(functools.partial(kernel, (Z, Y, X, shard, sent, width, hc...  193 us

profile of v2, /device:TPU:0, one launch (start us, length us, event | category | flops | bytes accessed | tf_op | source)
XLA Modules:
  0.0 204.5 jit_solution(14010860139171708452)
XLA Ops:
  0.0 0.0 copy-start
  0.0 0.8 dynamic-slice_convert_fusion
  0.9 0.7 select_maximum_fusion.refs_10_
  1.5 0.9 slice.21
  2.4 0.9 slice.22
  3.3 0.9 slice.23
  4.2 0.9 slice.24
  5.1 0.8 concatenate.6.refs_7_
  5.9 1.0 reshape.20
  6.9 0.7 reshape.21.refs_9_
  7.6 0.0 copy-done
  7.6 0.1 pad.12
  7.7 1.5 copy.13.refs_8_
  9.2 192.6 %shard_map.100 = bf16[256,2176]{1,0:T(8,128)(2,1)} custom-call(bf16[264,768]{1,0:T(8,128)(2,1)} %refs_0_.1, bf16[264,768]{1,0:T(8,128)(2,1)} %refs_1_.1, bf16[264,768]{1,0:T(8,128)(2,1)} %refs_2_.1, bf16[264,264]{1,0:T(8,128)(2,1)} %refs_3_.1, bf16[264,264]{1,0:T(8,128)(2,1)} %refs_4_.1, bf16[264,264]{1,0:T(8,128)(2,1)} %refs_5_.1, ...), custom_call_target="tpu_custom_call" | custom-call | tf_op jit(solution)/shard_map/pallas_call | solution.py:443
  201.8 1.7 copy.14
  203.4 1.1 slice.30
  (4 shorter events, 0.0 us)
Async XLA Ops:
  0.0 7.6 %copy-start = (bf16[256,2112]{0,1:T(8,128)(2,1)S(1)}, bf16[256,2112]{0,1:T(8,128)(2,1)}, u32[]{:S(2)}) copy-start(bf16[256,2112]{0,1:T(8,128)(2,1)} %param.10) | copy-start | bytes 3244036

commit v3 on v2

--- a/solution.py
+++ b/solution.py
@@ -287,10 +287,12 @@
         return jnp.concatenate([q[0], q[2], q[1], q[3]], axis=0)
 
     def mixer():
+        wait_across(K3)
         edge = main + 128
         n = swapped(normed[...].reshape(rows, Dp))
         outer_inner = jnp.dot(n, g3[...], preferred_element_type=F32)
         outer_inner = outer_inner.astype(BF16).astype(F32)
+        steps_a(False)
         value_rest = jnp.dot(n, g4[:, 0:edge], preferred_element_type=F32)
         value_rest = value_rest.astype(BF16).astype(F32)
         rest = value_rest[:, main:]
@@ -342,19 +344,20 @@
         zsteps(k)
         if k + 2 <= K3:
             own(k + 2)
-        if k + 2 == K3:
+        if k == 0:
             across(K4, z, go)
-        if k > 0:
-            wait_across(k - 1)
-            ffn_chunk(k - 1, k == 1)
+        if k == 1 and nff > 2:
+            wait_across(0)
+            ffn_chunk(0, True)
+    start_a()
     zsteps(K3)
-    start_a()
     steps_a(True)
+    for k in range(1 if nff > 2 else 0, nff - 1):
+        wait_across(k)
+        ffn_chunk(k, k == 0)
     wait_across(nff - 1)
     reduce(0, last_chunk, stream_ref, 1, 0.5)
     norm_to(res.at[0], 2)
-    wait_across(K3)
-    steps_a(False)
     mixer()
     reduce(1, mixer_block, res.at[0], 3, 1.0)
     norm_to(res.at[1], 4)

time: 205 us -> 205 us (level)
  no operation moved by 1% of the time
where the time goes in v3:
time: 205 us
  Pallas kernels  193 us (94%)
  local copies, waits for them, and re-layouts  10.4 us (5%)
    pallas_call x1, Pallas kernels, local(): pl.pallas_call(functools.partial(kernel, (Z, Y, X, shard, sent, width, hc...  193 us

profile of v3, /device:TPU:0, one launch (start us, length us, event | category | flops | bytes accessed | tf_op | source)
XLA Modules:
  0.0 204.7 jit_solution(13568211465195175091)
XLA Ops:
  0.0 0.0 copy-start
  0.0 0.8 dynamic-slice_convert_fusion
  0.9 0.7 select_maximum_fusion.refs_10_
  1.5 0.9 slice.21
  2.4 0.9 slice.22
  3.3 0.9 slice.23
  4.2 0.9 slice.24
  5.1 0.8 concatenate.6.refs_7_
  5.9 1.0 reshape.20
  6.9 0.7 reshape.21.refs_9_
  7.6 0.0 copy-done
  7.6 0.1 pad.12
  7.7 1.5 copy.13.refs_8_
  9.2 192.8 %shard_map.100 = bf16[256,2176]{1,0:T(8,128)(2,1)} custom-call(bf16[264,768]{1,0:T(8,128)(2,1)} %refs_0_.1, bf16[264,768]{1,0:T(8,128)(2,1)} %refs_1_.1, bf16[264,768]{1,0:T(8,128)(2,1)} %refs_2_.1, bf16[264,264]{1,0:T(8,128)(2,1)} %refs_3_.1, bf16[264,264]{1,0:T(8,128)(2,1)} %refs_4_.1, bf16[264,264]{1,0:T(8,128)(2,1)} %refs_5_.1, ...), custom_call_target="tpu_custom_call" | custom-call | tf_op jit(solution)/shard_map/pallas_call | solution.py:446
  202.0 1.7 copy.14
  203.7 1.1 slice.30
  (4 shorter events, 0.0 us)
Async XLA Ops:
  0.0 7.6 %copy-start = (bf16[256,2112]{0,1:T(8,128)(2,1)S(1)}, bf16[256,2112]{0,1:T(8,128)(2,1)}, u32[]{:S(2)}) copy-start(bf16[256,2112]{0,1:T(8,128)(2,1)} %param.10) | copy-start | bytes 3244036
